TPU v7x, 32 devices: a whole 2x2x4 slice. The times are simulated.
32 devices in a mesh: sp: 4 (over y, core), dp: 8 (over z, x).
Axes of the slice: x: 2, y: 2, z: 4, core: 2. Of those that a mesh axis runs over, the one named last changes fastest.
Arguments:
- q_latent: bfloat16 [8, 512, 512], P('dp', 'sp'), may hold values from -70 to 70
- kv_latent: bfloat16 [8, 512, 512], P('dp', 'sp'), may hold values from -70 to 70
- rope_key: bfloat16 [8, 512, 64], P('dp', 'sp'), may hold values from -370 to 370
- w_query: bfloat16 [512, 3072], P(None, 'dp'), may hold values from -0.25 to 0.25
- w_keyval: bfloat16 [512, 4096], P(None, 'sp'), may hold values from -0.25 to 0.25
- w_out: bfloat16 [2048, 2048], replicated, may hold values from -0.125 to 0.125
- query_gain: bfloat16 [512], replicated, may hold values from 0.099609375 to 1.8984375
- latent_gain: bfloat16 [512], replicated, may hold values from 0.099609375 to 1.8984375
- out_gain: bfloat16 [2048], replicated, may hold values from 0.099609375 to 1.8984375
Outputs:
- output: bfloat16 [8, 512, 2048], P('dp', 'sp')
All inputs are finite; a program needn't handle non-finite values.
Results may differ from a plain program's by a relative error of at most 0.03.
The roundings to bfloat16 on the way count: a program that leaves them out, or rounds other values in their place, can miss the bound.
Values may be sent and summed in bfloat16 or wider, within the bound.
A program may use at most 64 MiB of HBM per device.

v0:
```python
import jax
import jax.numpy as jnp
from jax import lax
from jax.sharding import PartitionSpec as P

H = 16
NOPE = 128
ROPE = 64
VDIM = 128


def normalize(row_values, gain_vector):
    widened = row_values.astype(jnp.float32)
    return (
        widened
        * lax.rsqrt(jnp.mean(widened * widened, axis=-1, keepdims=True) + 1e-05)
        * gain_vector.astype(jnp.float32)
    )


def angles_for(positions, rope_width):
    half_width = rope_width // 2
    inverse = 10000.0 ** (-jnp.arange(half_width, dtype=jnp.float32) / half_width)
    return positions.astype(jnp.float32)[:, None] * inverse[None, :]


def turn(vectors, angles):
    half_width = vectors.shape[-1] // 2
    cosine = jnp.cos(angles)
    sine_value = jnp.sin(angles)
    low_half = vectors[..., :half_width]
    high_half = vectors[..., half_width:]
    return jnp.concatenate(
        [low_half * cosine - high_half * sine_value, high_half * cosine + low_half * sine_value],
        axis=-1,
    )


def attend(query_head, keyval_head, rope_all):
    length = query_head.shape[0]
    local_heads = query_head.shape[1] // (NOPE + ROPE)
    query_three = query_head.reshape(length, local_heads, NOPE + ROPE)
    keyval_three = keyval_head.reshape(length, local_heads, NOPE + VDIM)
    block_rows = min(512, length)
    score_scale = (NOPE + ROPE) ** (-0.5)
    pieces = []
    for block_index in range(length // block_rows):
        block_start = block_index * block_rows
        block_stop = block_start + block_rows
        query_block = query_three[block_start:block_stop]
        scores = jnp.einsum(
            "qhd,khd->hqk",
            query_block[..., :NOPE],
            keyval_three[:block_stop, :, :NOPE],
            preferred_element_type=jnp.float32,
        )
        scores = scores + jnp.einsum(
            "qhr,kr->hqk",
            query_block[..., NOPE:],
            rope_all[:block_stop],
            preferred_element_type=jnp.float32,
        )
        scores = scores * score_scale
        allowed = jnp.arange(block_stop)[None, :] <= (block_start + jnp.arange(block_rows))[:, None]
        scores = jnp.where(allowed[None], scores, -jnp.inf)
        row_top = jnp.max(scores, axis=-1, keepdims=True)
        exponent = jnp.exp(scores - row_top)
        row_total = jnp.sum(exponent, axis=-1)
        summed = jnp.einsum(
            "hqk,khd->qhd",
            exponent.astype(jnp.bfloat16),
            keyval_three[:block_stop, :, NOPE:],
            preferred_element_type=jnp.float32,
        )
        pieces.append((summed / jnp.transpose(row_total)[:, :, None]).astype(jnp.bfloat16))
    return jnp.concatenate(pieces, axis=0).reshape(length, local_heads * VDIM)


def per_device(
    q_latent, kv_latent, rope_key, w_query, w_keyval, w_out, query_gain, latent_gain, out_gain
):
    tokens_here = q_latent.shape[1]
    offset = lax.axis_index("sp") * tokens_here
    positions = offset + jnp.arange(tokens_here, dtype=jnp.int32)
    angles = angles_for(positions, ROPE)
    query_norm = normalize(q_latent[0], query_gain).astype(jnp.bfloat16)
    query_raw = jnp.dot(
        query_norm,
        lax.all_gather(w_query, "dp", axis=1, tiled=True),
        preferred_element_type=jnp.float32,
    )
    query_raw = query_raw.reshape(tokens_here, H, NOPE + ROPE)
    queries = jnp.concatenate(
        [query_raw[..., :NOPE], turn(query_raw[..., NOPE:], angles[:, None, :])], axis=-1
    )
    queries = queries.astype(jnp.bfloat16).reshape(tokens_here, H * (NOPE + ROPE))
    latent_norm = normalize(kv_latent[0], latent_gain).astype(jnp.bfloat16)
    rope_turned = turn(rope_key[0].astype(jnp.float32), angles).astype(jnp.bfloat16)
    query_head = lax.all_to_all(queries, "sp", split_axis=1, concat_axis=0, tiled=True)
    latent_all, rope_all = (
        lax.all_gather(latent_norm, "sp", axis=0, tiled=True),
        lax.all_gather(rope_turned, "sp", axis=0, tiled=True),
    )
    keyval_head = jnp.dot(latent_all, w_keyval, preferred_element_type=jnp.float32).astype(
        jnp.bfloat16
    )
    attended = attend(query_head, keyval_head, rope_all)
    returned = lax.all_to_all(attended, "sp", split_axis=0, concat_axis=1, tiled=True)
    mixed_norm = normalize(returned, out_gain).astype(jnp.bfloat16)
    result = jnp.dot(mixed_norm, w_out, preferred_element_type=jnp.float32).astype(jnp.bfloat16)
    return result[None]


def solution(mesh):
    in_specs = (
        P("dp", "sp", None),
        P("dp", "sp", None),
        P("dp", "sp", None),
        P(None, "dp"),
        P(None, "sp"),
        P(),
        P(),
        P(),
        P(),
    )
    out_specs = P("dp", "sp", None)
    return jax.shard_map(
        per_device, mesh=mesh, in_specs=in_specs, out_specs=out_specs, check_vma=False
    )
```

profile of v0, /device:TPU:0, one launch (start us, length us, event | category | flops | bytes accessed | tf_op | source)
XLA Modules:
  0.0 132.7 jit_solution(3271215150385826949)
XLA Ops:
  6.5 0.0 copy-start
  6.5 0.0 copy-start.2
  6.5 0.0 all-gather.2.cloned.1.call-start
  6.5 0.7 all-gather.2.cloned.1.call-update
  7.3 0.7 convert_element_type.83
  7.9 0.7 convert_element_type.79
  8.6 1.0 fusion.23
  9.7 1.0 fusion.26
  10.7 1.0 fusion.28
  11.7 8.7 %all_gather.9 = bf16[512,512]{1,0:T(8,128)(2,1)S(1)} all-gather(bf16[128,512]{1,0:T(8,128)(2,1)S(1)} %fusion.28), channel_id=1, replica_groups=mesh['sp'=4,'dp'=8] {'sp'}, dimensions={0}, use_global_device_ids=true | all-gather | bytes 655360 | tf_op jit(solution)/shard_map/all_gather | solution.py:101
  20.4 0.7 bitcast_convert_fusion
  21.1 0.1 subtract_convert_fusion.1
  21.3 53.5 %all-gather.2.cloned.1.call-done = bf16[512,3072]{1,0:T(8,128)(2,1)} async-done(((bf16[512,384]{1,0:T(8,128)(2,1)}), bf16[512,3072]{1,0:T(8,128)(2,1)}) %all-gather.2.cloned.1.call-update) | async-done | bytes 3145744 | tf_op jit(solution)/shard_map/all_gather | solution.py:89
  74.8 4.7 %copy.23 = bf16[3072,512]{1,0:T(8,128)(2,1)} copy(bf16[3072,512]{0,1:T(8,128)(2,1)} %bitcast.53) | data formatting | bytes 6291456 | tf_op jit(solution)/shard_map/dot_general | solution.py:87
  79.5 0.0 copy-done.2
  79.5 2.9 %fusion.31 = f32[128,16,192]{0,2,1:T(8,128)S(1)} fusion(bf16[16,192,512]{2,1,0:T(8,128)(2,1)} %bitcast.52, bf16[1,128,512]{2,1,0:T(8,128)(2,1)S(1)} %copy-done.2, f32[512]{0:T(512)S(1)} %convert_element_type.83, f32[128]{0:T(128)S(1)} %add_rsqrt_fusion.1), kind=kOutput, calls=%fused_computation.39 | convolution fusion | flops 402915328 | bytes 4852224 | tf_op jit(solution)/shard_map/dot_general | solution.py:87
  82.4 0.1 slice.62
  82.5 0.1 subtract_convert_fusion
  82.6 1.0 pad_maximum_fusion
  83.6 3.5 %all-to-all-start = ((bf16[128,4,768]{0,2,1:T(8,128)(2,1)}), bf16[128,4,768]{0,2,1:T(8,128)(2,1)S(1)}, u32[]{:S(2)}, u32[]{:S(2)}) async-start(bf16[128,4,768]{0,2,1:T(8,128)(2,1)} %bitcast.6), calls=%async_computation | async-start | bytes 1572864 | tf_op jit(solution)/shard_map/all_to_all | solution.py:99
  87.1 0.0 copy-done
  87.1 1.7 %convolution_convert_fusion.1 = bf16[512,1024]{1,0:T(8,128)(2,1)} fusion(bf16[512,512]{1,0:T(8,128)(2,1)S(1)} %all_gather.9, bf16[512,1024]{1,0:T(8,128)(2,1)S(1)} %copy-done), kind=kOutput, calls=%fused_computation.10 | convolution fusion | flops 537395200 | bytes 2621440 | tf_op jit(solution)/shard_map/dot_general | solution.py:104
  88.8 1.9 %reshape.144 = bf16[512,4,256]{2,1,0:T(4,128)(2,1)S(1)} reshape(bf16[512,1024]{1,0:T(8,128)(2,1)} %convolution_convert_fusion.1) | data formatting | bytes 2097152 | tf_op jit(solution)/shard_map/reshape | solution.py:43
  90.7 9.2 %all_gather.11 = bf16[512,64]{0,1:T(8,128)(2,1)S(1)} all-gather(bf16[128,64]{0,1:T(8,128)(2,1)S(1)} %pad_maximum_fusion.1), channel_id=1, replica_groups=mesh['sp'=4,'dp'=8] {'sp'}, dimensions={0}, use_global_device_ids=true | all-gather | bytes 81920 | tf_op jit(solution)/shard_map/all_gather | solution.py:102
  99.9 0.8 iota_compare_fusion
  100.7 1.2 fusion.36
  101.8 0.0 all-to-all-done
  101.8 0.0 copy-start.1
  101.8 0.6 copy.24
  102.4 0.3 reshape.145
  102.7 0.7 fusion.19
  103.4 0.0 copy-done.1
  103.4 1.2 fusion.37
  104.6 0.0 copy-start.3
  104.6 0.6 fusion.2
  105.2 0.5 copy-done.3
  105.7 0.0 copy-start.4
  105.7 0.8 fusion.14
  106.5 0.1 all_to_all.22
  106.6 0.9 copy.28
  107.4 3.5 %all-to-all-start.1 = ((bf16[4,128,512]{1,2,0:T(8,128)(2,1)}), bf16[4,128,512]{1,2,0:T(8,128)(2,1)S(1)}, u32[]{:S(2)}, u32[]{:S(2)}) async-start(bf16[4,128,512]{1,2,0:T(8,128)(2,1)} %copy.28), calls=%async_computation.1 | async-start | bytes 1048576 | tf_op jit(solution)/shard_map/all_to_all | solution.py:108
  110.9 0.0 copy-done.4
  111.0 8.8 %all-to-all-done.1 = bf16[4,128,512]{1,2,0:T(8,128)(2,1)S(1)} async-done(((bf16[4,128,512]{1,2,0:T(8,128)(2,1)}), bf16[4,128,512]{1,2,0:T(8,128)(2,1)S(1)}, u32[]{:S(2)}, u32[]{:S(2)}) %all-to-all-start.1) | async-done | bytes 524320 | tf_op jit(solution)/shard_map/all_to_all | solution.py:108
  119.7 0.3 multiply_reduce_fusion
  120.0 0.3 fusion.18
  120.4 5.5 %fusion.4 = bf16[1,128,2048]{2,1,0:T(8,128)(2,1)} fusion(bf16[128,2048]{0,1:T(8,128)(2,1)S(1)} %fusion.18, bf16[2048,2048]{1,0:T(8,128)(2,1)} %param.14), kind=kOutput, calls=%fused_computation.7 | convolution fusion | flops 1074003968 | bytes 9437184 | tf_op jit(solution)/shard_map/dot_general | solution.py:110
  (7 shorter events, 0.0 us)
Async XLA Ops:
  6.5 80.6 %copy-start = (bf16[512,1024]{1,0:T(8,128)(2,1)S(1)}, bf16[512,1024]{1,0:T(8,128)(2,1)}, u32[]{:S(2)}) copy-start(bf16[512,1024]{1,0:T(8,128)(2,1)} %param.13) | copy-start | bytes 3145732
  6.5 73.0 %copy-start.2 = (bf16[1,128,512]{2,1,0:T(8,128)(2,1)S(1)}, bf16[1,128,512]{2,1,0:T(8,128)(2,1)}, u32[]{:S(2)}) copy-start(bf16[1,128,512]{2,1,0:T(8,128)(2,1)} %param.9) | copy-start | bytes 393220
  6.5 68.3 %all-gather.2.cloned.1.call-start = ((), (), s32[]{:S(2)}) async-start(), calls=%async_computation.2 | async-start | bytes 3538944 | tf_op jit(solution)/shard_map/all_gather | solution.py:89
  83.6 18.2 %all-to-all-start = ((bf16[128,4,768]{0,2,1:T(8,128)(2,1)}), bf16[128,4,768]{0,2,1:T(8,128)(2,1)S(1)}, u32[]{:S(2)}, u32[]{:S(2)}) async-start(bf16[128,4,768]{0,2,1:T(8,128)(2,1)} %bitcast.6), calls=%async_computation | async-start | bytes 1572864 | tf_op jit(solution)/shard_map/all_to_all | solution.py:99
  101.8 1.6 %copy-start.1 = (pred[512,512]{0,1:T(8,128)(4,1)S(1)}, pred[512,512]{0,1:T(8,128)(4,1)}, u32[]{:S(2)}) copy-start(pred[512,512]{0,1:T(8,128)(4,1)} %iota_compare_fusion) | copy-start | bytes 786436
  104.6 1.0 copy-start.3
  105.7 5.3 %copy-start.4 = (bf16[2048]{0:T(1024)(128)(2,1)S(1)}, bf16[2048]{0:T(1024)(128)(2,1)}, u32[]{:S(2)}) copy-start(bf16[2048]{0:T(1024)(128)(2,1)} %param.17) | copy-start | bytes 12292
  107.4 12.3 %all-to-all-start.1 = ((bf16[4,128,512]{1,2,0:T(8,128)(2,1)}), bf16[4,128,512]{1,2,0:T(8,128)(2,1)S(1)}, u32[]{:S(2)}, u32[]{:S(2)}) async-start(bf16[4,128,512]{1,2,0:T(8,128)(2,1)} %copy.28), calls=%async_computation.1 | async-start | bytes 1048576 | tf_op jit(solution)/shard_map/all_to_all | solution.py:108
Sparse Core Ops, SparseCore 0:
  9.4 65.3 all-gather.1
where the time goes:
time: 133 us
  waiting for transfers between devices  63 us (47%)
  blocking collectives  17.9 us (13%)
  between operations  13.6 us (10%)
  matrix products  12.7 us (10%)
  local copies, waits for them, and re-layouts  10.1 us (8%)
  other arithmetic  8.35 us (6%)
  starting transfers between devices  6.97 us (5%)
    all_gather x1, waiting for transfers between devices, per_device(): lax.all_gather(w_query, 'dp', axis=1, tiled=True)  53.5 us
    all_gather x1, blocking collectives, per_device(): lax.all_gather(rope_turned, 'sp', axis=0, tiled=True)  9.22 us
    all_to_all x1, waiting for transfers between devices, per_device(): lax.all_to_all(attended, 'sp', split_axis=0, concat_axis=1, tiled=True)  8.76 us
    all_gather x1, blocking collectives, per_device(): lax.all_gather(latent_norm, 'sp', axis=0, tiled=True)  8.68 us
    dot_general x1, matrix products, per_device(): jnp.dot(mixed_norm, w_out, preferred_element_type=jnp.float32)  5.47 us
    dot_general x1, local copies, waits for them, and re-layouts, per_device(): jnp.dot(query_norm, lax.all_gather(w_query, 'dp', axis=1, tiled=True), pr...  4.68 us
    all_to_all x1, starting transfers between devices, per_device(): lax.all_to_all(queries, 'sp', split_axis=1, concat_axis=0, tiled=True)  3.49 us
    all_to_all x1, starting transfers between devices, per_device(): lax.all_to_all(attended, 'sp', split_axis=0, concat_axis=1, tiled=True)  3.47 us
  transfers between devices with their start and end apart: 3, of which 2 were waited for; matrix products, arithmetic and copies ran while one was open for 8% of the time, Pallas kernels for 0%

commit v1 on v0

--- a/solution.py
+++ b/solution.py
@@ -105,7 +105,15 @@
         jnp.bfloat16
     )
     attended = attend(query_head, keyval_head, rope_all)
-    returned = lax.all_to_all(attended, "sp", split_axis=0, concat_axis=1, tiled=True)
+    returned = jnp.concatenate(
+        lax.all_to_all(
+            jnp.stack(jnp.split(attended, lax.psum(1, axis_name="sp"), 0)),
+            "sp",
+            split_axis=0,
+            concat_axis=0,
+        ),
+        1,
+    )
     mixed_norm = normalize(returned, out_gain).astype(jnp.bfloat16)
     result = jnp.dot(mixed_norm, w_out, preferred_element_type=jnp.float32).astype(jnp.bfloat16)
     return result[None]

time: 133 us -> 133 us (level)
  no operation moved by 1% of the time
where the time goes in v1:
time: 133 us
  waiting for transfers between devices  63 us (47%)
  blocking collectives  17.9 us (13%)
  between operations  13.6 us (10%)
  matrix products  12.7 us (10%)
  local copies, waits for them, and re-layouts  9.27 us (7%)
  other arithmetic  9.21 us (7%)
  starting transfers between devices  6.97 us (5%)
    all_gather x1, waiting for transfers between devices, per_device(): lax.all_gather(w_query, 'dp', axis=1, tiled=True)  53.5 us
    all_gather x1, blocking collectives, per_device(): lax.all_gather(rope_turned, 'sp', axis=0, tiled=True)  9.23 us
    all_to_all x1, waiting for transfers between devices, per_device(): lax.all_to_all(jnp.stack(jnp.split(attended, lax.psum(1, axis_name='sp'),...  8.76 us
    all_gather x1, blocking collectives, per_device(): lax.all_gather(latent_norm, 'sp', axis=0, tiled=True)  8.68 us
    dot_general x1, matrix products, per_device(): jnp.dot(mixed_norm, w_out, preferred_element_type=jnp.float32)  5.47 us
    dot_general x1, local copies, waits for them, and re-layouts, per_device(): jnp.dot(query_norm, lax.all_gather(w_query, 'dp', axis=1, tiled=True), pr...  4.68 us
    all_to_all x1, starting transfers between devices, per_device(): lax.all_to_all(queries, 'sp', split_axis=1, concat_axis=0, tiled=True)  3.49 us
    all_to_all x1, starting transfers between devices, per_device(): lax.all_to_all(jnp.stack(jnp.split(attended, lax.psum(1, axis_name='sp'),...  3.47 us
  transfers between devices with their start and end apart: 3, of which 2 were waited for; matrix products, arithmetic and copies ran while one was open for 8% of the time, Pallas kernels for 0%

profile of v1, /device:TPU:0, one launch (start us, length us, event | category | flops | bytes accessed | tf_op | source)
XLA Modules:
  0.0 132.7 jit_solution(4825476354346039712)
XLA Ops:
  6.5 0.0 copy-start
  6.5 0.0 copy-start.2
  6.5 0.0 all-gather.2.cloned.1.call-start
  6.5 0.7 all-gather.2.cloned.1.call-update
  7.3 0.7 convert_element_type.83
  7.9 0.7 convert_element_type.79
  8.6 1.0 fusion.23
  9.7 1.0 fusion.26
  10.7 1.0 fusion.28
  11.7 8.7 %all_gather.9 = bf16[512,512]{1,0:T(8,128)(2,1)S(1)} all-gather(bf16[128,512]{1,0:T(8,128)(2,1)S(1)} %fusion.28), channel_id=1, replica_groups=mesh['sp'=4,'dp'=8] {'sp'}, dimensions={0}, use_global_device_ids=true | all-gather | bytes 655360 | tf_op jit(solution)/shard_map/all_gather | solution.py:101
  20.4 0.7 bitcast_convert_fusion
  21.1 0.1 subtract_convert_fusion.1
  21.3 53.5 %all-gather.2.cloned.1.call-done = bf16[512,3072]{1,0:T(8,128)(2,1)} async-done(((bf16[512,384]{1,0:T(8,128)(2,1)}), bf16[512,3072]{1,0:T(8,128)(2,1)}) %all-gather.2.cloned.1.call-update) | async-done | bytes 3145744 | tf_op jit(solution)/shard_map/all_gather | solution.py:89
  74.8 4.7 %copy.22 = bf16[3072,512]{1,0:T(8,128)(2,1)} copy(bf16[3072,512]{0,1:T(8,128)(2,1)} %bitcast.55) | data formatting | bytes 6291456 | tf_op jit(solution)/shard_map/dot_general | solution.py:87
  79.5 0.0 copy-done.2
  79.5 2.9 %fusion.31 = f32[128,16,192]{0,2,1:T(8,128)S(1)} fusion(bf16[16,192,512]{2,1,0:T(8,128)(2,1)} %bitcast.54, bf16[1,128,512]{2,1,0:T(8,128)(2,1)S(1)} %copy-done.2, f32[512]{0:T(512)S(1)} %convert_element_type.83, f32[128]{0:T(128)S(1)} %add_rsqrt_fusion.1), kind=kOutput, calls=%fused_computation.40 | convolution fusion | flops 402915328 | bytes 4852224 | tf_op jit(solution)/shard_map/dot_general | solution.py:87
  82.4 0.1 slice.66
  82.5 0.1 subtract_convert_fusion
  82.6 1.0 pad_maximum_fusion
  83.6 3.5 %all-to-all-start = ((bf16[128,4,768]{0,2,1:T(8,128)(2,1)}), bf16[128,4,768]{0,2,1:T(8,128)(2,1)S(1)}, u32[]{:S(2)}, u32[]{:S(2)}) async-start(bf16[128,4,768]{0,2,1:T(8,128)(2,1)} %bitcast.6), calls=%async_computation | async-start | bytes 1572864 | tf_op jit(solution)/shard_map/all_to_all | solution.py:99
  87.1 0.0 copy-done
  87.1 1.7 %convolution_convert_fusion.1 = bf16[512,1024]{1,0:T(8,128)(2,1)} fusion(bf16[512,512]{1,0:T(8,128)(2,1)S(1)} %all_gather.9, bf16[512,1024]{1,0:T(8,128)(2,1)S(1)} %copy-done), kind=kOutput, calls=%fused_computation.10 | convolution fusion | flops 537395200 | bytes 2621440 | tf_op jit(solution)/shard_map/dot_general | solution.py:104
  88.8 1.9 %reshape.150 = bf16[512,4,256]{2,1,0:T(4,128)(2,1)S(1)} reshape(bf16[512,1024]{1,0:T(8,128)(2,1)} %convolution_convert_fusion.1) | data formatting | bytes 2097152 | tf_op jit(solution)/shard_map/reshape | solution.py:43
  90.7 9.2 %all_gather.11 = bf16[512,64]{0,1:T(8,128)(2,1)S(1)} all-gather(bf16[128,64]{0,1:T(8,128)(2,1)S(1)} %pad_maximum_fusion.2), channel_id=1, replica_groups=mesh['sp'=4,'dp'=8] {'sp'}, dimensions={0}, use_global_device_ids=true | all-gather | bytes 81920 | tf_op jit(solution)/shard_map/all_gather | solution.py:102
  99.9 0.8 iota_compare_fusion
  100.7 1.2 fusion.36
  101.8 0.0 all-to-all-done
  101.8 0.0 copy-start.1
  101.8 0.6 copy.23
  102.4 0.3 reshape.151
  102.7 0.7 fusion.19
  103.4 0.0 copy-done.1
  103.4 1.2 fusion.38
  104.6 0.0 copy-start.3
  104.6 0.6 fusion.2
  105.2 0.5 copy-done.3
  105.7 0.0 copy-start.4
  105.7 0.8 fusion.14
  106.5 0.1 fusion.37
  106.6 0.9 pad_maximum_fusion.1
  107.4 3.5 %all-to-all-start.1 = ((bf16[4,128,512]{1,2,0:T(8,128)(2,1)}), bf16[4,128,512]{1,2,0:T(8,128)(2,1)S(1)}, u32[]{:S(2)}, u32[]{:S(2)}) async-start(bf16[4,128,512]{1,2,0:T(8,128)(2,1)} %pad_maximum_fusion.1), calls=%async_computation.1 | async-start | bytes 1048576 | tf_op jit(solution)/shard_map/all_to_all | solution.py:109
  110.9 0.0 copy-done.4
  110.9 8.8 %all-to-all-done.1 = bf16[4,128,512]{1,2,0:T(8,128)(2,1)S(1)} async-done(((bf16[4,128,512]{1,2,0:T(8,128)(2,1)}), bf16[4,128,512]{1,2,0:T(8,128)(2,1)S(1)}, u32[]{:S(2)}, u32[]{:S(2)}) %all-to-all-start.1) | async-done | bytes 524320 | tf_op jit(solution)/shard_map/all_to_all | solution.py:109
  119.7 0.3 multiply_reduce_fusion
  120.0 0.3 fusion.18
  120.3 5.5 %fusion.4 = bf16[1,128,2048]{2,1,0:T(8,128)(2,1)} fusion(bf16[128,2048]{0,1:T(8,128)(2,1)S(1)} %fusion.18, bf16[2048,2048]{1,0:T(8,128)(2,1)} %param.14), kind=kOutput, calls=%fused_computation.7 | convolution fusion | flops 1074003968 | bytes 9437184 | tf_op jit(solution)/shard_map/dot_general | solution.py:118
  (7 shorter events, 0.0 us)
Async XLA Ops:
  6.5 80.6 %copy-start = (bf16[512,1024]{1,0:T(8,128)(2,1)S(1)}, bf16[512,1024]{1,0:T(8,128)(2,1)}, u32[]{:S(2)}) copy-start(bf16[512,1024]{1,0:T(8,128)(2,1)} %param.13) | copy-start | bytes 3145732
  6.5 73.0 %copy-start.2 = (bf16[1,128,512]{2,1,0:T(8,128)(2,1)S(1)}, bf16[1,128,512]{2,1,0:T(8,128)(2,1)}, u32[]{:S(2)}) copy-start(bf16[1,128,512]{2,1,0:T(8,128)(2,1)} %param.9) | copy-start | bytes 393220
  6.5 68.3 %all-gather.2.cloned.1.call-start = ((), (), s32[]{:S(2)}) async-start(), calls=%async_computation.2 | async-start | bytes 3538944 | tf_op jit(solution)/shard_map/all_gather | solution.py:89
  83.6 18.2 %all-to-all-start = ((bf16[128,4,768]{0,2,1:T(8,128)(2,1)}), bf16[128,4,768]{0,2,1:T(8,128)(2,1)S(1)}, u32[]{:S(2)}, u32[]{:S(2)}) async-start(bf16[128,4,768]{0,2,1:T(8,128)(2,1)} %bitcast.6), calls=%async_computation | async-start | bytes 1572864 | tf_op jit(solution)/shard_map/all_to_all | solution.py:99
  101.8 1.6 %copy-start.1 = (pred[512,512]{0,1:T(8,128)(4,1)S(1)}, pred[512,512]{0,1:T(8,128)(4,1)}, u32[]{:S(2)}) copy-start(pred[512,512]{0,1:T(8,128)(4,1)} %iota_compare_fusion) | copy-start | bytes 786436
  104.6 1.0 copy-start.3
  105.7 5.3 %copy-start.4 = (bf16[2048]{0:T(1024)(128)(2,1)S(1)}, bf16[2048]{0:T(1024)(128)(2,1)}, u32[]{:S(2)}) copy-start(bf16[2048]{0:T(1024)(128)(2,1)} %param.17) | copy-start | bytes 12292
  107.4 12.3 %all-to-all-start.1 = ((bf16[4,128,512]{1,2,0:T(8,128)(2,1)}), bf16[4,128,512]{1,2,0:T(8,128)(2,1)S(1)}, u32[]{:S(2)}, u32[]{:S(2)}) async-start(bf16[4,128,512]{1,2,0:T(8,128)(2,1)} %pad_maximum_fusion.1), calls=%async_computation.1 | async-start | bytes 1048576 | tf_op jit(solution)/shard_map/all_to_all | solution.py:109
Sparse Core Ops, SparseCore 0:
  9.4 65.3 all-gather.1
